TPU v7x, 32 devices: a whole 2x2x4 slice. The times are simulated.
32 devices in a mesh: grp: 2 (over y), ep: 8 (over z, core), tp: 2 (over x).
Axes of the slice: x: 2, y: 2, z: 4, core: 2. Of those that a mesh axis runs over, the one named last changes fastest.
Arguments:
- mixer_tokens: bfloat16 [4096, 2048], P(('grp', 'ep', 'tp')), parts along dimension 0, may hold values from -6 to 6
- mixer_gain: float32 [2048], replicated, may hold values from 0.1 to 1.9
- proj_in: bfloat16 [2048, 1024], P(None, 'tp'), may hold values from -0.125 to 0.125
- pool_weight: bfloat16 [4, 256, 256], P('tp'), may hold values from -0.375 to 0.375
- pool_scale: float32 [1024], P('tp'), may hold values from 0.1 to 1.9
- proj_out: bfloat16 [1024, 2048], P('tp'), may hold values from -0.1875 to 0.1875
- expert_tokens: bfloat16 [4096, 2048], P(('grp', 'ep', 'tp')), parts along dimension 0, may hold values from -6 to 6
- expert_gain: float32 [2048], replicated, may hold values from 0.1 to 1.9
- expert_route: int32 [4096, 2], P(('grp', 'ep')), parts along dimension 0, may hold values from 0 to 15, as said below
- route_gate: float32 [4096, 2], P(('grp', 'ep')), parts along dimension 0, may hold values from 0.1 to 1
- expert_gate: bfloat16 [16, 2048, 1024], P('ep', None, 'tp'), may hold values from -0.125 to 0.125
- expert_up: bfloat16 [16, 2048, 1024], P('ep', None, 'tp'), may hold values from -0.125 to 0.125
- expert_down: bfloat16 [16, 1024, 2048], P('ep', 'tp'), may hold values from -0.1875 to 0.1875
Outputs:
- mixed_rows: bfloat16 [4096, 2048], P(('grp', 'ep', 'tp')), parts along dimension 0
- moe_rows: bfloat16 [4096, 2048], P(('grp', 'ep', 'tp')), parts along dimension 0
There are 2 independent parts, one for each index of `grp`. A program takes and returns all parts, laid end to end along the dimension named above; an argument that names none is the same for every part. Nothing has to cross between parts.
Inputs may be any that keep to these rules, and one draw needn't show every extreme that they name: `expert_route`: each row names two different experts of one group of 4 consecutive experts. In each aligned block of 128 rows (the routes of the tokens that lie on one device) no expert is named by more than 32 rows, and every expert of a group that the block names at all is named by exactly 32 of its rows; one group, the same in every block, is named in every block, and which other groups a block names varies from block to block.
All inputs are finite; a program needn't handle non-finite values.
Results may differ from a plain program's by a relative error of at most 0.011.
Values may be sent and summed in bfloat16 or wider, within the bound.
A program may use at most 128 MiB of HBM per device.

v0:
```python
import jax
import jax.numpy as jnp
from jax import lax
from jax.sharding import PartitionSpec as P

GROUP_SIZE = 4


norm_eps = 1e-05
rim_rows = 15


def shifted(value, axis, by):
    peers = lax.axis_size(axis)
    pairs = [(i, i + by) for i in range(peers) if 0 <= i + by < peers]
    return lax.ppermute(value, axis, pairs)


def layer_norm(values, norm_gain):
    widened = values.astype(jnp.float32)
    center = jnp.mean(widened, axis=-1, keepdims=True)
    spread = jnp.mean(jnp.square(widened - center), axis=-1, keepdims=True)
    return ((widened - center) * lax.rsqrt(spread + norm_eps) * norm_gain).astype(jnp.bfloat16)


def pooled_diff(extended, windows, first_row):
    widened = extended.astype(jnp.float32)
    row_total = widened.shape[0] - rim_rows
    own_rows = widened[rim_rows:]
    window_sum = own_rows
    for offset in range(1, rim_rows + 1):
        lagged = widened[rim_rows - offset : rim_rows - offset + row_total]
        window_sum = window_sum + jnp.where(offset < windows[None, :], lagged, 0.0)
    position = first_row + jnp.arange(row_total, dtype=jnp.int32)
    covered = jnp.minimum(position[:, None] + 1, windows[None, :]).astype(jnp.float32)
    return (window_sum / covered - own_rows).astype(jnp.bfloat16)


def pool_mix(projected, pool_weight, pool_scale, windows, first_row):
    prior = shifted(projected[-rim_rows:], "ep", 1)
    differences = pooled_diff(jnp.concatenate([prior, projected], axis=0), windows, first_row)
    row_total, local_width = differences.shape
    grouped = differences.reshape(row_total, pool_weight.shape[0], pool_weight.shape[1])
    mixed_groups = jnp.einsum(
        "tgc,gcd->tgd", grouped, pool_weight, preferred_element_type=jnp.float32
    )
    return (mixed_groups.reshape(row_total, local_width) * pool_scale).astype(jnp.bfloat16)


def route_table(routes, experts, capacity):
    flat_route = routes.reshape(-1)
    onehot = (flat_route[:, None] == jnp.arange(experts, dtype=jnp.int32)[None, :]).astype(
        jnp.int32
    )
    earlier = jnp.cumsum(onehot, axis=0) - onehot
    rank_in = jnp.sum(earlier * onehot, axis=1)
    placed = flat_route * capacity + rank_in
    token_mark = jnp.arange(flat_route.shape[0], dtype=jnp.int32) // 2 + 1
    sender = jnp.zeros((experts * capacity,), jnp.int32).at[placed].set(token_mark)
    return (placed, sender)


def fill_slots(rows_here, sender):
    picked = rows_here[jnp.maximum(sender - 1, 0)]
    return jnp.where((sender > 0)[:, None], picked, jnp.zeros_like(picked))


def lift_rows(slot_rows, expert_gate, expert_up):
    gate_part = jnp.einsum(
        "pesd,edh->pesh", slot_rows, expert_gate, preferred_element_type=jnp.float32
    )
    up_part = jnp.einsum("pesd,edh->pesh", slot_rows, expert_up, preferred_element_type=jnp.float32)
    return (jax.nn.silu(gate_part) * up_part).astype(jnp.bfloat16)


def lower_rows(hidden, expert_down):
    return jnp.einsum("pesh,ehd->pesd", hidden, expert_down, preferred_element_type=jnp.float32)


def shards(
    mixer_tokens,
    mixer_gain,
    proj_in,
    pool_weight,
    pool_scale,
    proj_out,
    expert_tokens,
    expert_gain,
    expert_route,
    route_gate,
    expert_gate,
    expert_up,
    expert_down,
):
    ep_count = lax.axis_size("ep")
    tp_index = lax.axis_index("tp")
    ep_index = lax.axis_index("ep")
    own_count = mixer_tokens.shape[0]
    model_width = mixer_tokens.shape[1]
    local_width = proj_in.shape[1]
    group_width = pool_weight.shape[1]
    experts = expert_gate.shape[0] * ep_count
    capacity = own_count * GROUP_SIZE // experts
    channel = tp_index * local_width + jnp.arange(local_width, dtype=jnp.int32)
    windows = jnp.left_shift(jnp.full_like(channel, 2), channel // group_width)
    normed_mixer = layer_norm(mixer_tokens, mixer_gain)
    normed_expert = layer_norm(expert_tokens, expert_gain)
    own_start = tp_index * own_count
    own_gates = lax.dynamic_slice_in_dim(route_gate, own_start, own_count, 0)
    projected = jnp.dot(
        lax.all_gather(normed_mixer, "tp", axis=0, tiled=True),
        proj_in,
        preferred_element_type=jnp.float32,
    ).astype(jnp.bfloat16)
    shard_count = projected.shape[0]
    pooled = pool_mix(projected, pool_weight, pool_scale, windows, ep_index * shard_count)
    mixed_rows = lax.psum_scatter(
        jnp.dot(pooled, proj_out, preferred_element_type=jnp.float32).astype(jnp.bfloat16),
        "tp",
        scatter_dimension=0,
        tiled=True,
    )
    own_route = lax.dynamic_slice_in_dim(expert_route, own_start, own_count, 0)
    placed, sender = route_table(own_route, experts, capacity)
    outgoing = fill_slots(normed_expert, sender).reshape(ep_count, -1, capacity, model_width)
    hidden = lift_rows(
        lax.all_gather(
            lax.all_to_all(outgoing, "ep", split_axis=0, concat_axis=0, tiled=True),
            "tp",
            axis=0,
            tiled=True,
        ),
        expert_gate,
        expert_up,
    )
    summed = lax.psum_scatter(
        lower_rows(hidden, expert_down).astype(jnp.bfloat16), "tp", scatter_dimension=0, tiled=True
    )
    returned = lax.all_to_all(summed, "ep", split_axis=0, concat_axis=0, tiled=True)
    expert_out = returned.reshape(-1, model_width)[placed].reshape(own_count, 2, model_width)
    moe_rows = jnp.sum(own_gates[:, :, None] * expert_out.astype(jnp.float32), axis=1).astype(
        jnp.bfloat16
    )
    return (mixed_rows, moe_rows)


def solution(mesh):
    return jax.shard_map(
        shards,
        mesh=mesh,
        in_specs=(
            P(("grp", "ep", "tp"), None),
            P(),
            P(None, "tp"),
            P("tp", None, None),
            P("tp"),
            P("tp", None),
            P(("grp", "ep", "tp"), None),
            P(),
            P(("grp", "ep"), None),
            P(("grp", "ep"), None),
            P("ep", None, "tp"),
            P("ep", None, "tp"),
            P("ep", "tp", None),
        ),
        out_specs=(P(("grp", "ep", "tp"), None), P(("grp", "ep", "tp"), None)),
        check_vma=False,
    )
```

profile of v0, /device:TPU:0, one launch (start us, length us, event | category | flops | bytes accessed | tf_op | source)
XLA Modules:
  0.0 298.6 jit_solution(15637397274559170409)
XLA Ops:
  7.2 0.0 all-gather.5.cloned.1.call-start
  7.2 0.8 broadcast_multiply_fusion
  8.1 0.1 copy.32
  8.2 0.1 eq.29
  8.3 0.1 eq.25
  8.5 0.6 reduce-window.6
  9.1 0.2 slice_reduce_fusion
  9.3 0.1 copy.31
  9.4 0.1 mul.95
  9.6 0.1 fusion.51
  9.7 1.4 scatter_custom_fusion
  11.1 1.2 convert_reduce_fusion
  12.3 1.3 fusion.20
  13.6 0.1 broadcast_in_dim.161
  13.7 1.4 fusion.22
  15.1 3.3 %gather_fusion = bf16[512,2048]{1,0:T(8,128)(2,1)} fusion(bf16[128,2048]{1,0:T(8,128)(2,1)S(1)} %fusion.22, s32[1024]{0:T(1024)S(1)} %pad_clamp_fusion.1), kind=kCustom, calls=%fused_computation | custom fusion | bytes 4196352 | tf_op jit(solution)/shard_map/gather | solution.py:64
  18.5 1.8 broadcast_select_fusion
  20.3 55.2 %all_to_all.10 = bf16[8,2,32,2048]{3,2,1,0:T(8,128)(2,1)S(1)} all-to-all(bf16[8,2,32,2048]{3,2,1,0:T(8,128)(2,1)S(1)} %broadcast_select_fusion), channel_id=1, replica_groups=mesh['grp'=2,'ep'=8,'tp'=2] {'ep'}, dimensions={0} | all-to-all | bytes 4194304 | tf_op jit(solution)/shard_map/all_to_all | solution.py:128
  75.5 1.5 copy.35
  77.0 0.0 reduce-scatter.8.cloned.1.call-start
  77.0 55.8 %all-gather.5.cloned.1.call-done = bf16[16,2,32,2048]{3,2,0,1:T(8,128)(2,1)} async-done(((bf16[8,2,32,2048]{3,2,0,1:T(8,128)(2,1)}), bf16[16,2,32,2048]{3,2,0,1:T(8,128)(2,1)}) %all-gather.5.cloned.1.call-update) | async-done | bytes 4194320 | tf_op jit(solution)/shard_map/all_gather | solution.py:127
  132.8 7.2 %fusion.2 = f32[2,16,32,512]{3,2,1,0:T(8,128)} fusion(bf16[16,2,32,2048]{3,2,0,1:T(8,128)(2,1)} %all-gather.5.cloned.1.call-done, bf16[2,2048,512]{2,1,0:T(8,128)(2,1)} %param.24), kind=kOutput, calls=%fused_computation.5 | convolution fusion | flops 2147483648 | bytes 10485760 | tf_op jit(solution)/shard_map/pesd,edh->pesh/dot_general | solution.py:72
  140.0 11.9 %convert_bitcast_fusion = bf16[16,2,32,2048]{3,2,0,1:T(8,128)(2,1)} fusion(bf16[2,512,2048]{2,1,0:T(8,128)(2,1)} %param.25, f32[2,16,32,512]{3,2,1,0:T(8,128)} %fusion.2, bf16[16,2,32,2048]{3,2,0,1:T(8,128)(2,1)} %all-gather.5.cloned.1.call-done, bf16[2,2048,512]{2,1,0:T(8,128)(2,1)} %param.23), kind=kOutput, calls=%fused_computation.9 | convolution fusion | flops 4300210176 | bytes 18874368 | tf_op jit(solution)/shard_map/pesh,ehd->pesd/dot_general | solution.py:77
  151.9 2.5 copy.41
  154.4 4.2 %copy.45 = bf16[2,8,64,2048]{3,1,2,0:T(8,128)(2,1)} copy(bf16[2,8,64,2048]{3,2,1,0:T(8,128)(2,1)S(1)} %bitcast.94) | data formatting | bytes 8388608
  158.7 0.2 all-gather.3.cloned.1.call-start
  158.9 0.8 copy-done.1
  159.7 0.2 convert_reduce_fusion.1
  159.8 0.3 fusion.23
  160.1 1.2 fusion.25
  161.5 51.7 %reduce-scatter.8.cloned.1.call-done = bf16[8,131072]{1,0:T(8,128)(2,1)} async-done(((bf16[16,131072]{1,0:T(8,128)(2,1)}), bf16[8,131072]{1,0:T(8,128)(2,1)}) %reduce-scatter.8.cloned.1.call-update) | async-done | bytes 2097168
  213.2 4.1 %copy.46 = bf16[1,8,64,2048]{3,2,1,0:T(8,128)(2,1)} copy(bf16[1,8,64,2048]{3,1,2,0:T(8,128)(2,1)} %bitcast.97) | data formatting | bytes 4194304
  217.3 4.6 %all-to-all-start.1 = ((bf16[8,2,32,2048]{3,2,1,0:T(8,128)(2,1)}), bf16[8,2,32,2048]{3,2,1,0:T(8,128)(2,1)}, u32[]{:S(2)}, u32[]{:S(2)}) async-start(bf16[8,2,32,2048]{3,2,1,0:T(8,128)(2,1)} %bitcast.96), calls=%async_computation.2 | async-start | bytes 4194304 | tf_op jit(solution)/shard_map/all_to_all | solution.py:139
  221.9 14.7 %all-gather.3.cloned.1.call-done = bf16[256,2048]{1,0:T(8,128)(2,1)} async-done(((bf16[128,2048]{1,0:T(8,128)(2,1)}), bf16[256,2048]{1,0:T(8,128)(2,1)}) %all-gather.3.cloned.1.call-update) | async-done | bytes 1048592 | tf_op jit(solution)/shard_map/all_gather | solution.py:111
  236.6 2.6 convolution_convert_fusion.1
  239.3 1.6 collective-permute-start
  240.9 0.8 collective-permute-done
  241.7 0.1 maximum_convert_fusion
  241.8 1.1 fusion.45
  242.9 0.3 fusion.46
  243.2 0.1 fusion.44
  243.3 1.7 convolution_convert_fusion
  245.1 0.1 copy.30
  245.2 25.8 %all-to-all-done.1 = bf16[8,2,32,2048]{3,2,1,0:T(8,128)(2,1)} async-done(((bf16[8,2,32,2048]{3,2,1,0:T(8,128)(2,1)}), bf16[8,2,32,2048]{3,2,1,0:T(8,128)(2,1)}, u32[]{:S(2)}, u32[]{:S(2)}) %all-to-all-start.1) | async-done | bytes 2097184 | tf_op jit(solution)/shard_map/all_to_all | solution.py:139
  271.0 4.2 %gather_fusion.1 = bf16[256,2048]{1,0:T(8,128)(2,1)S(1)} fusion(bf16[512,2048]{1,0:T(8,128)(2,1)} %bitcast.15, s32[1024]{0:T(1024)S(1)} %pad_clamp_fusion), kind=kCustom, calls=%fused_computation.1 | custom fusion | bytes 2098176 | tf_op jit(solution)/shard_map/gather | solution.py:140
  275.3 2.4 reshape.188
  277.6 5.6 %multiply_reduce_fusion = bf16[128,2048]{1,0:T(8,128)(2,1)} fusion(f32[128,2,2048]{2,1,0:T(2,128)} %reshape.188, f32[128,2]{1,0:T(8,128)S(1)} %copy.30), kind=kLoop, calls=%fused_computation.18 | loop fusion | flops 786432 | bytes 2622464 | tf_op jit(solution)/shard_map/reduce_sum | solution.py:141
  283.2 8.9 %reduce-scatter.6.cloned.1.call-done = bf16[128,2048]{1,0:T(8,128)(2,1)} async-done(((bf16[256,2048]{1,0:T(8,128)(2,1)}), bf16[128,2048]{1,0:T(8,128)(2,1)}) %reduce-scatter.6.cloned.1.call-update) | async-done | bytes 524304 | tf_op jit(solution)/shard_map/reduce_scatter | solution.py:117
  (41 shorter events, 0.4 us)
Async XLA Ops:
  7.2 236.2 %copy-start = (bf16[512,2048]{1,0:T(8,128)(2,1)S(1)}, bf16[512,2048]{1,0:T(8,128)(2,1)}, u32[]{:S(2)}) copy-start(bf16[512,2048]{1,0:T(8,128)(2,1)} %param.18) | copy-start | bytes 6291460
  7.2 125.6 %all-gather.5.cloned.1.call-start = ((), (), s32[]{:S(2)}) async-start(), calls=%async_computation.6 | async-start | bytes 6291456 | tf_op jit(solution)/shard_map/all_gather | solution.py:127
  77.0 136.2 %reduce-scatter.8.cloned.1.call-start = ((), (), s32[]{:S(2)}) async-start(), calls=%async_computation.7 | async-start | bytes 6291456
  158.6 1.0 copy-start.1
  158.6 1.5 copy-start.3
  158.7 78.0 %all-gather.3.cloned.1.call-start = ((), (), s32[]{:S(2)}) async-start(), calls=%async_computation.4 | async-start | bytes 1572864 | tf_op jit(solution)/shard_map/all_gather | solution.py:111
  217.3 53.7 %all-to-all-start.1 = ((bf16[8,2,32,2048]{3,2,1,0:T(8,128)(2,1)}), bf16[8,2,32,2048]{3,2,1,0:T(8,128)(2,1)}, u32[]{:S(2)}, u32[]{:S(2)}) async-start(bf16[8,2,32,2048]{3,2,1,0:T(8,128)(2,1)} %bitcast.96), calls=%async_computation.2 | async-start | bytes 4194304 | tf_op jit(solution)/shard_map/all_to_all | solution.py:139
  221.9 70.2 %reduce-scatter.6.cloned.1.call-start = ((), (), s32[]{:S(2)}) async-start(), calls=%async_computation.5 | async-start | bytes 1572864 | tf_op jit(solution)/shard_map/reduce_scatter | solution.py:117
  239.3 2.4 collective-permute-start
  241.7 1.1 copy-start.2
  241.8 1.4 copy-start.4
  243.3 1.7 copy-start.5
Sparse Core Ops, SparseCore 0:
  77.1 55.6 all-gather.4
  158.8 54.3 reduce-scatter.7
  215.3 21.2 all-gather.2
  245.2 46.8 reduce-scatter.5
where the time goes:
time: 299 us
  waiting for transfers between devices  158 us (53%)
  blocking collectives  55.2 us (18%)
  local copies, waits for them, and re-layouts  25.5 us (9%)
  matrix products  23.7 us (8%)
  other arithmetic  16 us (5%)
  between operations  14 us (5%)
  starting transfers between devices  6.52 us (2%)
    all_gather x1, waiting for transfers between devices, shards(): lax.all_gather(lax.all_to_all(outgoing, 'ep', split_axis=0, concat_axis=0...  55.8 us
    all_to_all x1, blocking collectives, shards(): lax.all_to_all(outgoing, 'ep', split_axis=0, concat_axis=0, tiled=True)  55.2 us
    unnamed x5, waiting for transfers between devices  51.8 us
    all_to_all x1, waiting for transfers between devices, shards(): lax.all_to_all(summed, 'ep', split_axis=0, concat_axis=0, tiled=True)  25.8 us
    all_gather x1, waiting for transfers between devices, shards(): lax.all_gather(normed_mixer, 'tp', axis=0, tiled=True)  14.7 us
    dot_general x1, matrix products, lower_rows(): jnp.einsum('pesh,ehd->pesd', hidden, expert_down, preferred_element_type=...  11.9 us
    unnamed x15, local copies, waits for them, and re-layouts  11.6 us
    reduce_scatter x1, waiting for transfers between devices, shards(): lax.psum_scatter(jnp.dot(pooled, proj_out, preferred_element_type=jnp.flo...  8.89 us
  transfers between devices with their start and end apart: 6, of which 6 were waited for; matrix products, arithmetic and copies ran while one was open for 8% of the time, Pallas kernels for 0%

commit v1 on v0

v1 whole, which is shorter than its diff:
```python
import functools

import jax
import jax.numpy as jnp
from jax import lax
from jax.experimental import pallas as pl
from jax.experimental.pallas import tpu as pltpu
from jax.sharding import PartitionSpec as P

GROUP_SIZE = 4
MARK = 128
HALO = 16

norm_eps = 1e-05
MESH = pl.DeviceIdType.MESH
f32, bf16 = jnp.float32, jnp.bfloat16


def norm_rows(src, gain, store, step=16):
    def body(i, _):
        rows = pl.ds(pl.multiple_of(i * step, step), step)
        v = src[rows, :].astype(f32)
        center = jnp.mean(v, axis=-1, keepdims=True)
        v = v - center
        spread = jnp.mean(jnp.square(v), axis=-1, keepdims=True)
        store(rows, (v * lax.rsqrt(spread + norm_eps) * gain[...]).astype(bf16))
        return 0

    lax.fori_loop(0, src.shape[0] // step, body, 0)


def kernel(
    dims,
    mixer, mgain, proj_in, pool_w, pool_s, proj_out,
    tokens, egain, route, gate, wgate, wup, wdown,
    mixed, moe,
    w_in, w_pool, w_out, w_g, w_u, w_d,
    aug, mark, out, xs, hid, po, rd, sx, rx, sz, ret,
    mx, ext, mo, mr,
    s_w, s_z, r_z, s_x, r_x, s_d, r_d, s_o, r_o, s_p, r_p, s_b, r_b,
    s_m, r_m, s_h, r_h, s_q, r_q,
):
    nz, duo, nx, slots, own, d = dims
    ep, x = lax.axis_index("ep"), lax.axis_index("tp")
    n_ep = nz * duo
    z, c = ep // duo, lax.rem(ep, duo)
    mate = z * duo + (duo - 1 - c)
    nxt, prv = lax.rem(ep + 1, n_ep), lax.rem(ep + n_ep - 1, n_ep)

    def xpeer(k):
        return lax.rem(x + k, nx)

    def zpeer(k):
        return lax.rem(z + k, nz)

    def remote(src, dst, ssem, rsem, e, t):
        return pltpu.make_async_remote_copy(
            src_ref=src, dst_ref=dst, send_sem=ssem, recv_sem=rsem,
            device_id={"ep": e, "tp": t}, device_id_type=MESH)

    loads = [
        pltpu.make_async_copy(a, b, s_w.at[i])
        for i, (a, b) in enumerate(
            [(proj_in, w_in), (pool_w, w_pool), (proj_out, w_out), (wgate, w_g), (wup, w_u), (wdown, w_d)])
    ]
    for cp in loads:
        cp.start()

    barrier = pltpu.get_barrier_semaphore()

    def greet(e, t):
        pl.semaphore_signal(barrier, inc=1, device_id={"ep": e, "tp": t}, device_id_type=MESH)

    for k in range(1, nz):
        greet(zpeer(k) * duo + c, x)
    for k in range(1, nx):
        greet(ep, xpeer(k))
    greet(mate, x)
    greet(nxt, x)
    greet(prv, x)

    def keep_tokens(rows, v):
        aug[rows, pl.ds(0, d)] = v

    norm_rows(tokens, egain, keep_tokens)
    base = pl.ds(pl.multiple_of(x * own, own), own)
    rt = route[base, :]
    gt = gate[base, :]
    lane = lax.broadcasted_iota(jnp.int32, (own, MARK), 1)
    r0, r1 = rt[:, 0:1], rt[:, 1:2]
    i0, i1 = lax.rem(r0, GROUP_SIZE), lax.rem(r1, GROUP_SIZE)
    g0, g1 = gt[:, 0:1], gt[:, 1:2]
    head = jnp.where(lane == i0, g0, 0.0) + jnp.where(lane == i1, g1, 0.0)
    tail = jnp.where(lane == i0 + GROUP_SIZE, g0, 0.0) + jnp.where(lane == i1 + GROUP_SIZE, g1, 0.0)
    rest = tail - tail.astype(bf16).astype(f32)
    aug[:, pl.ds(d, MARK)] = (head + rest).astype(bf16)
    member = (lane == r0 // GROUP_SIZE).astype(f32)
    row = lax.broadcasted_iota(jnp.int32, (own, own), 0)
    col = lax.broadcasted_iota(jnp.int32, (own, own), 1)
    before = jnp.dot((col < row).astype(f32).astype(bf16), member.astype(bf16), preferred_element_type=f32)
    place = jnp.sum(member * (before + (lane * slots).astype(f32)), axis=-1, keepdims=True).astype(jnp.int32)
    slot = lax.broadcasted_iota(jnp.int32, (own, nz * slots), 1)
    mark[...] = (slot == place).astype(f32).astype(bf16)
    packed = lax.dot_general(
        mark[...], aug[...], (((0,), (0,)), ((), ())), preferred_element_type=f32
    ).astype(bf16)
    out[...] = packed.reshape(nz, slots, d + MARK)

    pl.semaphore_wait(barrier, nz - 1 + nx - 1 + 3)

    def send_z(k):
        g = zpeer(nz - k)
        return remote(out.at[g], xs.at[z, c, x], s_z.at[k], r_z.at[z], g * duo + c, x)

    def fwd_x(k, j):
        zs = zpeer(k)
        return remote(xs.at[zs, c, x], xs.at[zs, c, x], s_x.at[k, j], r_x.at[zs, x], ep, xpeer(j))

    def fwd_d(k, j):
        zs, xp = zpeer(k), xpeer(j)
        return remote(xs.at[zs, c, xp], xs.at[zs, c, xp], s_d.at[k, j], r_d.at[zs, xp], mate, x)

    def pair(k):
        zs = zpeer(k)
        return remote(po.at[zs, duo - 1 - c], rd.at[zs], s_o.at[k], r_o.at[zs], mate, x)

    def sum_x(k, j):
        zs, xp = zpeer(k), xpeer(j)
        return remote(sx.at[zs, xp], rx.at[zs, x], s_p.at[k, j], r_p.at[zs, x], ep, xp)

    def back(k):
        zs = zpeer(k)
        return remote(sz.at[zs], ret.at[z], s_b.at[k], r_b.at[z], zs * duo + c, x)

    def mix_x(j):
        return remote(mx.at[x], mx.at[x], s_m.at[j], r_m.at[x], ep, xpeer(j))

    def rim():
        return remote(ext.at[pl.ds(nx * own, HALO)], ext.at[pl.ds(0, HALO)], s_h, r_h, nxt, x)

    def mix_out(j):
        xp = xpeer(j)
        return remote(mo.at[xp], mr.at[x], s_q.at[j], r_q.at[x], ep, xp)

    def arrived(dst, rsem):
        remote(dst, dst, s_h, rsem, ep, xpeer(1)).wait_recv()

    for k in range(1, nz):
        send_z(k).start()
    xs[z, c, x] = out[z]

    def keep_mixer(rows, v):
        mx[x, rows, :] = v

    norm_rows(mixer, mgain, keep_mixer)
    for j in range(1, nx):
        mix_x(j).start()

    def mixer_project():
        for j in range(1, nx):
            arrived(mx.at[xpeer(j)], r_m.at[xpeer(j)])
        loads[0].wait()
        rows = mx[...].reshape(nx * own, d)
        ext[pl.ds(HALO, nx * own), :] = jnp.dot(rows, w_in[...], preferred_element_type=f32).astype(bf16)
        rim().start()

    def mixer_finish():
        arrived(ext.at[pl.ds(0, HALO)], r_h)
        loads[1].wait()
        loads[2].wait()
        groups, width = w_pool.shape[0], w_pool.shape[1]
        rows = nx * own
        at = ep * rows + lax.broadcasted_iota(jnp.int32, (rows, width), 0)
        total = None
        for g in range(groups):
            cols = pl.ds(g * width, width)
            v = ext[:, cols].astype(f32)
            r = lax.broadcasted_iota(jnp.int32, v.shape, 0)
            v = jnp.where((r < HALO) & (ep == 0), 0.0, v)
            group = x * groups + g
            s, window, picked = v, 1, None
            for level in range(groups * nx):
                s = s + pltpu.roll(s, window, 0)
                window *= 2
                picked = s if picked is None else jnp.where(group == level, s, picked)
            w = lax.shift_left(jnp.int32(2), group)
            covered = jnp.minimum(at + 1, w).astype(f32)
            diff = (picked[HALO:] / covered - v[HALO:]).astype(bf16)
            m = jnp.dot(diff, w_pool[g], preferred_element_type=f32) * pool_s[:, cols]
            part = jnp.dot(m.astype(bf16), w_out[cols, :], preferred_element_type=f32)
            total = part if total is None else total + part
        mo[...] = total.astype(bf16).reshape(nx, own, d)
        for j in range(1, nx):
            mix_out(j).start()

    def compute(k):
        zs = zpeer(k)
        for j in range(nx):
            arrived(xs.at[zs, duo - 1 - c, xpeer(j)], r_d.at[zs, xpeer(j)])
        rows = duo * nx * slots
        block = xs[zs, :, :, :, pl.ds(0, d)].reshape(rows, d)
        side = xs[zs, :, :, :, pl.ds(d, MARK)].reshape(rows, MARK).astype(f32)
        lanes = lax.broadcasted_iota(jnp.int32, (rows, MARK), 1)
        held, width = w_g.shape[0], w_g.shape[2]
        for e in range(held):
            a = jnp.dot(block, w_g[e], preferred_element_type=f32)
            b = jnp.dot(block, w_u[e], preferred_element_type=f32)
            i = c * held + e
            w = jnp.sum(jnp.where((lanes == i) | (lanes == i + GROUP_SIZE), side, 0.0), axis=-1, keepdims=True)
            hid[:, pl.ds(e * width, width)] = (a / (1.0 + jnp.exp(-a)) * b * w).astype(bf16)
        po[zs] = jnp.dot(hid[...], w_d[...], preferred_element_type=f32).astype(bf16).reshape(duo, nx, slots, d)
        pair(k).start()

    def step(t, _):
        @pl.when(t < nz)
        def _():
            zs = zpeer(t)

            @pl.when(t > 0)
            def _():
                arrived(xs.at[zs, c, x], r_z.at[zs])

            for j in range(1, nx):
                fwd_x(t, j).start()
            fwd_d(t, 0).start()

        @pl.when((t >= 1) & (t < nz + 1))
        def _():
            k = t - 1
            for j in range(1, nx):
                arrived(xs.at[zpeer(k), c, xpeer(j)], r_x.at[zpeer(k), xpeer(j)])
                fwd_d(k, j).start()

        @pl.when(t == 2)
        def _():
            mixer_project()
            for cp in loads[3:]:
                cp.wait()

        @pl.when(t == 3)
        def _():
            mixer_finish()

        @pl.when((t >= 2) & (t < nz + 2))
        def _():
            compute(t - 2)

        @pl.when((t >= 3) & (t < nz + 3))
        def _():
            k = t - 3
            zs = zpeer(k)
            arrived(rd.at[zs], r_o.at[zs])
            sx[zs] = (po[zs, c].astype(f32) + rd[zs].astype(f32)).astype(bf16)
            for j in range(1, nx):
                sum_x(k, j).start()

        @pl.when(t >= 4)
        def _():
            k = t - 4
            zs = zpeer(k)
            total = sx[zs, x].astype(f32)
            for j in range(1, nx):
                arrived(rx.at[zs, xpeer(j)], r_p.at[zs, xpeer(j)])
                total = total + rx[zs, xpeer(j)].astype(f32)

            @pl.when(k == 0)
            def _():
                ret[z] = total.astype(bf16)

            @pl.when(k > 0)
            def _():
                sz[zs] = total.astype(bf16)
                back(k).start()

        return 0

    lax.fori_loop(0, nz + 4, step, 0)

    total = mo[x].astype(f32)
    for j in range(1, nx):
        arrived(mr.at[xpeer(j)], r_q.at[xpeer(j)])
        total = total + mr[xpeer(j)].astype(f32)
    mixed[...] = total.astype(bf16)

    for k in range(1, nz):
        arrived(ret.at[zpeer(k)], r_b.at[zpeer(k)])
    moe[...] = jnp.dot(mark[...], ret[...].reshape(nz * slots, d), preferred_element_type=f32).astype(bf16)

    rim().wait_send()
    for j in range(1, nx):
        mix_x(j).wait_send()
        mix_out(j).wait_send()
    for k in range(nz):
        if k:
            send_z(k).wait_send()
            back(k).wait_send()
        pair(k).wait_send()
        for j in range(nx):
            fwd_d(k, j).wait_send()
            if j:
                fwd_x(k, j).wait_send()
                sum_x(k, j).wait_send()


def shards(
    mixer_tokens, mixer_gain, proj_in, pool_weight, pool_scale, proj_out,
    expert_tokens, expert_gain, expert_route, route_gate, expert_gate, expert_up, expert_down,
):
    own, d = mixer_tokens.shape
    held, _, width = expert_gate.shape
    nx = lax.axis_size("tp")
    duo = GROUP_SIZE // held
    nz = lax.axis_size("ep") // duo
    experts = held * lax.axis_size("ep")
    slots = (own * GROUP_SIZE // experts) * GROUP_SIZE // 2
    dims = (nz, duo, nx, slots, own, d)
    vmem, anyspace = pl.BlockSpec(memory_space=pltpu.VMEM), pl.BlockSpec(memory_space=pl.ANY)
    dma = pltpu.SemaphoreType.DMA
    down = expert_down.reshape(held * width, d)
    local = proj_in.shape[1]
    V = pltpu.VMEM
    scratch = [
        V(proj_in.shape, bf16), V(pool_weight.shape, bf16), V(proj_out.shape, bf16),
        V(expert_gate.shape, bf16), V(expert_up.shape, bf16), V(down.shape, bf16),
        V((own, d + MARK), bf16), V((own, nz * slots), bf16), V((nz, slots, d + MARK), bf16),
        V((nz, duo, nx, slots, d + MARK), bf16), V((duo * nx * slots, held * width), bf16),
        V((nz, duo, nx, slots, d), bf16), V((nz, nx, slots, d), bf16),
        V((nz, nx, slots, d), bf16), V((nz, nx, slots, d), bf16),
        V((nz, slots, d), bf16), V((nz, slots, d), bf16),
        V((nx, own, d), bf16), V((HALO + nx * own, local), bf16),
        V((nx, own, d), bf16), V((nx, own, d), bf16),
        dma((6,)), dma((nz,)), dma((nz,)),
        dma((nz, nx)), dma((nz, nx)), dma((nz, nx)), dma((nz, nx)),
        dma((nz,)), dma((nz,)), dma((nz, nx)), dma((nz, nx)), dma((nz,)), dma((nz,)),
        dma((nx,)), dma((nx,)), dma, dma, dma((nx,)), dma((nx,)),
    ]
    return pl.pallas_call(
        functools.partial(kernel, dims),
        out_shape=(
            jax.ShapeDtypeStruct((own, d), bf16),
            jax.ShapeDtypeStruct((own, d), bf16),
        ),
        in_specs=[
            vmem, vmem, anyspace, anyspace, vmem, anyspace,
            vmem, vmem, vmem, vmem, anyspace, anyspace, anyspace,
        ],
        out_specs=(vmem, vmem),
        scratch_shapes=scratch,
        compiler_params=pltpu.CompilerParams(
            collective_id=0, has_side_effects=True, vmem_limit_bytes=62 * 1024 * 1024,
        ),
    )(
        mixer_tokens, mixer_gain.reshape(1, d), proj_in, pool_weight, pool_scale.reshape(1, local), proj_out,
        expert_tokens, expert_gain.reshape(1, d), expert_route, route_gate, expert_gate, expert_up, down,
    )


def solution(mesh):
    return jax.shard_map(
        shards,
        mesh=mesh,
        in_specs=(
            P(("grp", "ep", "tp"), None),
            P(),
            P(None, "tp"),
            P("tp", None, None),
            P("tp"),
            P("tp", None),
            P(("grp", "ep", "tp"), None),
            P(),
            P(("grp", "ep"), None),
            P(("grp", "ep"), None),
            P("ep", None, "tp"),
            P("ep", None, "tp"),
            P("ep", "tp", None),
        ),
        out_specs=(P(("grp", "ep", "tp"), None), P(("grp", "ep", "tp"), None)),
        check_vma=False,
    )
```

time: 299 us -> 100 us (0.33)
  waiting for transfers between devices: 158 us -> 0 us
  Pallas kernels: 0 us -> 91.8 us
  blocking collectives: 55.2 us -> 0 us
  matrix products: 23.7 us -> 0 us
  local copies, waits for them, and re-layouts: 25.5 us -> 6.71 us
  other arithmetic: 16 us -> 0 us
  between operations: 14 us -> 0.64 us
  starting transfers between devices: 6.52 us -> 0 us
    pallas_call x0 -> x1, Pallas kernels: none -> 91.8 us  [shards(): pl.pallas_call(functools.partial(kernel, dims), out_shape=(jax.ShapeDtype...]
    all_gather x2 -> x0, waiting for transfers between devices: 70.5 us -> none  [the longest x1 55.8 us: shards(): lax.all_gather(lax.all_to_all(outgoing, 'ep', split_axis=0, concat_axis=0...]
    all_to_all x1 -> x0, blocking collectives: 55.2 us -> none  [shards(): lax.all_to_all(outgoing, 'ep', split_axis=0, concat_axis=0, tiled=True)]
    unnamed x5 -> x0, waiting for transfers between devices: 51.8 us -> none
    all_to_all x1 -> x0, waiting for transfers between devices: 25.8 us -> none  [shards(): lax.all_to_all(summed, 'ep', split_axis=0, concat_axis=0, tiled=True)]
    dot_general x5 -> x0, matrix products: 23.7 us -> none  [the longest x1 11.9 us: lower_rows(): jnp.einsum('pesh,ehd->pesd', hidden, expert_down, preferred_element_type=...]
    reduce_scatter x1 -> x0, waiting for transfers between devices: 8.89 us -> none  [shards(): lax.psum_scatter(jnp.dot(pooled, proj_out, preferred_element_type=jnp.flo...]
    reduce_sum x6 -> x0, other arithmetic: 8.65 us -> none  [the longest x1 5.59 us: shards(): jnp.sum(own_gates[:, :, None] * expert_out.astype(jnp.float32), axis=1)]
  transfers between devices with their start and end apart: 6 -> 0, of which waited for: 6 -> 0; matrix products, arithmetic and copies ran while one was open for 8% -> 0% of each run, Pallas kernels for 0% -> 0%
where the time goes in v1:
time: 100 us; the launch traced here: 99.2 us
  Pallas kernels  91.8 us (92%)
  local copies, waits for them, and re-layouts  6.71 us (7%)
    pallas_call x1, Pallas kernels, shards(): pl.pallas_call(functools.partial(kernel, dims), out_shape=(jax.ShapeDtype...  91.8 us
    unnamed x4, local copies, waits for them, and re-layouts  6.71 us

profile of v1, /device:TPU:0, one launch (start us, length us, event | category | flops | bytes accessed | tf_op | source)
XLA Modules:
  0.0 99.2 jit_solution(13395162578178996096)
XLA Ops:
  0.6 1.5 %copy.15.route = s32[256,2]{1,0:T(8,128)} copy(s32[256,2]{0,1:T(2,128)} %param.21) | data formatting | bytes 4096 | tf_op args[8]
  2.1 1.5 %copy.16.gate = f32[256,2]{1,0:T(8,128)} copy(f32[256,2]{0,1:T(2,128)} %param.22) | data formatting | bytes 4096 | tf_op args[9]
  3.6 91.8 %shard_map.140 = (bf16[128,2048]{1,0:T(8,128)(2,1)}, bf16[128,2048]{1,0:T(8,128)(2,1)}) custom-call(bf16[128,2048]{1,0:T(8,128)(2,1)} %mixer.1, f32[1,2048]{1,0:T(1,128)} %bitcast.5, bf16[2048,512]{1,0:T(8,128)(2,1)} %proj_in.1, bf16[2,256,256]{2,1,0:T(8,128)(2,1)} %pool_w.1, f32[1,512]{1,0:T(1,128)} %bitcast.7, bf16[512,2048]{1,0:T(8,128)(2,1)} %proj_out.1, ...), custom_call_target="tpu_custom_call" | custom-call | tf_op jit(solution)/shard_map/pallas_call | solution.py:337
  95.4 1.9 %copy.19 = bf16[128,2048]{1,0:T(8,128)(2,1)} copy(bf16[128,2048]{1,0:T(8,128)(2,1)} %get-tuple-element.4) | data formatting | bytes 1048576
  97.3 1.9 %copy.20 = bf16[128,2048]{1,0:T(8,128)(2,1)} copy(bf16[128,2048]{1,0:T(8,128)(2,1)} %get-tuple-element.5) | data formatting | bytes 1048576

commit v2 on v1

--- a/solution.py
+++ b/solution.py
@@ -10,6 +10,7 @@
 GROUP_SIZE = 4
 MARK = 128
 HALO = 16
+PARTS = 2
 
 norm_eps = 1e-05
 MESH = pl.DeviceIdType.MESH
@@ -35,12 +36,13 @@
     tokens, egain, route, gate, wgate, wup, wdown,
     mixed, moe,
     w_in, w_pool, w_out, w_g, w_u, w_d,
-    aug, mark, out, xs, hid, po, rd, sx, rx, sz, ret,
+    turn, aug, mark, out, xs, hid, po, rd, sx, rx, sz, ret,
     mx, ext, mo, mr,
     s_w, s_z, r_z, s_x, r_x, s_d, r_d, s_o, r_o, s_p, r_p, s_b, r_b,
     s_m, r_m, s_h, r_h, s_q, r_q,
 ):
-    nz, duo, nx, slots, own, d = dims
+    nz, parts, duo, nx, slots, own, d = dims
+    units = nz * parts
     ep, x = lax.axis_index("ep"), lax.axis_index("tp")
     n_ep = nz * duo
     z, c = ep // duo, lax.rem(ep, duo)
@@ -52,6 +54,12 @@
 
     def zpeer(k):
         return lax.rem(z + k, nz)
+
+    def unit(k):
+        return zpeer(k // parts) * parts + lax.rem(k, parts)
+
+    def mine(k):
+        return z * parts + lax.rem(k, parts)
 
     def remote(src, dst, ssem, rsem, e, t):
         return pltpu.make_async_remote_copy(
@@ -79,17 +87,65 @@
     greet(nxt, x)
     greet(prv, x)
 
+    def send_z(k):
+        g = zpeer(nz - k // parts)
+        piece = g * parts + lax.rem(k, parts)
+        return remote(out.at[piece], xs.at[mine(k), c, x], s_z.at[k], r_z.at[mine(k)], g * duo + c, x)
+
+    def fwd_x(k, j):
+        zs = unit(k)
+        return remote(xs.at[zs, c, x], xs.at[zs, c, x], s_x.at[k, j], r_x.at[zs, x], ep, xpeer(j))
+
+    def fwd_d(k, j):
+        zs, xp = unit(k), xpeer(j)
+        return remote(xs.at[zs, c, xp], xs.at[zs, c, xp], s_d.at[k, j], r_d.at[zs, xp], mate, x)
+
+    def pair(k):
+        zs = unit(k)
+        return remote(po.at[zs, duo - 1 - c], rd.at[zs], s_o.at[k], r_o.at[zs], mate, x)
+
+    def sum_x(k, j):
+        zs, xp = unit(k), xpeer(j)
+        return remote(sx.at[zs, xp], rx.at[zs, x], s_p.at[k, j], r_p.at[zs, x], ep, xp)
+
+    def back(k):
+        zs = unit(k)
+        return remote(sz.at[zs], ret.at[mine(k)], s_b.at[k], r_b.at[mine(k)], zpeer(k // parts) * duo + c, x)
+
+    def mix_x(j):
+        return remote(mx.at[x], mx.at[x], s_m.at[j], r_m.at[x], ep, xpeer(j))
+
+    def rim():
+        return remote(ext.at[pl.ds(nx * own, HALO)], ext.at[pl.ds(0, HALO)], s_h, r_h, nxt, x)
+
+    def mix_out(j, h):
+        xp, half = xpeer(j), pl.ds(h * (own // 2), own // 2)
+        return remote(mo.at[xp, half], mr.at[x, half], s_q.at[j, h], r_q.at[x, h], ep, xp)
+
+    def arrived(dst, rsem):
+        remote(dst, dst, s_h, rsem, ep, xpeer(1)).wait_recv()
+
+    def keep_mixer(rows, v):
+        mx[x, rows, :] = v
+
+    norm_rows(mixer, mgain, keep_mixer)
+    pl.semaphore_wait(barrier, nz - 1 + nx - 1 + 3)
+    for j in range(1, nx):
+        mix_x(j).start()
+
     def keep_tokens(rows, v):
         aug[rows, pl.ds(0, d)] = v
 
     norm_rows(tokens, egain, keep_tokens)
     base = pl.ds(pl.multiple_of(x * own, own), own)
-    rt = route[base, :]
-    gt = gate[base, :]
+    turn[...] = jnp.zeros_like(turn)
+    turn[0:2, :] = route[:, base].astype(f32)
+    turn[2:4, :] = gate[:, base]
+    columns = turn[...].T
     lane = lax.broadcasted_iota(jnp.int32, (own, MARK), 1)
-    r0, r1 = rt[:, 0:1], rt[:, 1:2]
+    r0, r1 = columns[:, 0:1].astype(jnp.int32), columns[:, 1:2].astype(jnp.int32)
     i0, i1 = lax.rem(r0, GROUP_SIZE), lax.rem(r1, GROUP_SIZE)
-    g0, g1 = gt[:, 0:1], gt[:, 1:2]
+    g0, g1 = columns[:, 2:3], columns[:, 3:4]
     head = jnp.where(lane == i0, g0, 0.0) + jnp.where(lane == i1, g1, 0.0)
     tail = jnp.where(lane == i0 + GROUP_SIZE, g0, 0.0) + jnp.where(lane == i1 + GROUP_SIZE, g1, 0.0)
     rest = tail - tail.astype(bf16).astype(f32)
@@ -98,63 +154,18 @@
     row = lax.broadcasted_iota(jnp.int32, (own, own), 0)
     col = lax.broadcasted_iota(jnp.int32, (own, own), 1)
     before = jnp.dot((col < row).astype(f32).astype(bf16), member.astype(bf16), preferred_element_type=f32)
-    place = jnp.sum(member * (before + (lane * slots).astype(f32)), axis=-1, keepdims=True).astype(jnp.int32)
-    slot = lax.broadcasted_iota(jnp.int32, (own, nz * slots), 1)
+    place = jnp.sum(member * (before + (lane * (parts * slots)).astype(f32)), axis=-1, keepdims=True).astype(jnp.int32)
+    slot = lax.broadcasted_iota(jnp.int32, (own, units * slots), 1)
     mark[...] = (slot == place).astype(f32).astype(bf16)
     packed = lax.dot_general(
         mark[...], aug[...], (((0,), (0,)), ((), ())), preferred_element_type=f32
     ).astype(bf16)
-    out[...] = packed.reshape(nz, slots, d + MARK)
-
-    pl.semaphore_wait(barrier, nz - 1 + nx - 1 + 3)
-
-    def send_z(k):
-        g = zpeer(nz - k)
-        return remote(out.at[g], xs.at[z, c, x], s_z.at[k], r_z.at[z], g * duo + c, x)
-
-    def fwd_x(k, j):
-        zs = zpeer(k)
-        return remote(xs.at[zs, c, x], xs.at[zs, c, x], s_x.at[k, j], r_x.at[zs, x], ep, xpeer(j))
-
-    def fwd_d(k, j):
-        zs, xp = zpeer(k), xpeer(j)
-        return remote(xs.at[zs, c, xp], xs.at[zs, c, xp], s_d.at[k, j], r_d.at[zs, xp], mate, x)
-
-    def pair(k):
-        zs = zpeer(k)
-        return remote(po.at[zs, duo - 1 - c], rd.at[zs], s_o.at[k], r_o.at[zs], mate, x)
-
-    def sum_x(k, j):
-        zs, xp = zpeer(k), xpeer(j)
-        return remote(sx.at[zs, xp], rx.at[zs, x], s_p.at[k, j], r_p.at[zs, x], ep, xp)
-
-    def back(k):
-        zs = zpeer(k)
-        return remote(sz.at[zs], ret.at[z], s_b.at[k], r_b.at[z], zs * duo + c, x)
-
-    def mix_x(j):
-        return remote(mx.at[x], mx.at[x], s_m.at[j], r_m.at[x], ep, xpeer(j))
-
-    def rim():
-        return remote(ext.at[pl.ds(nx * own, HALO)], ext.at[pl.ds(0, HALO)], s_h, r_h, nxt, x)
-
-    def mix_out(j):
-        xp = xpeer(j)
-        return remote(mo.at[xp], mr.at[x], s_q.at[j], r_q.at[x], ep, xp)
-
-    def arrived(dst, rsem):
-        remote(dst, dst, s_h, rsem, ep, xpeer(1)).wait_recv()
-
-    for k in range(1, nz):
+    out[...] = packed.reshape(units, slots, d + MARK)
+
+    for k in range(parts, units):
         send_z(k).start()
-    xs[z, c, x] = out[z]
-
-    def keep_mixer(rows, v):
-        mx[x, rows, :] = v
-
-    norm_rows(mixer, mgain, keep_mixer)
-    for j in range(1, nx):
-        mix_x(j).start()
+    for k in range(parts):
+        xs[mine(k), c, x] = out[mine(k)]
 
     def mixer_project():
         for j in range(1, nx):
@@ -190,11 +201,9 @@
             part = jnp.dot(m.astype(bf16), w_out[cols, :], preferred_element_type=f32)
             total = part if total is None else total + part
         mo[...] = total.astype(bf16).reshape(nx, own, d)
-        for j in range(1, nx):
-            mix_out(j).start()
 
     def compute(k):
-        zs = zpeer(k)
+        zs = unit(k)
         for j in range(nx):
             arrived(xs.at[zs, duo - 1 - c, xpeer(j)], r_d.at[zs, xpeer(j)])
         rows = duo * nx * slots
@@ -212,11 +221,11 @@
         pair(k).start()
 
     def step(t, _):
-        @pl.when(t < nz)
-        def _():
-            zs = zpeer(t)
-
-            @pl.when(t > 0)
+        @pl.when(t < units)
+        def _():
+            zs = unit(t)
+
+            @pl.when(t >= parts)
             def _():
                 arrived(xs.at[zs, c, x], r_z.at[zs])
 
@@ -224,74 +233,90 @@
                 fwd_x(t, j).start()
             fwd_d(t, 0).start()
 
-        @pl.when((t >= 1) & (t < nz + 1))
+        @pl.when((t >= 1) & (t < units + 1))
         def _():
             k = t - 1
             for j in range(1, nx):
-                arrived(xs.at[zpeer(k), c, xpeer(j)], r_x.at[zpeer(k), xpeer(j)])
+                arrived(xs.at[unit(k), c, xpeer(j)], r_x.at[unit(k), xpeer(j)])
                 fwd_d(k, j).start()
 
-        @pl.when(t == 2)
-        def _():
-            mixer_project()
-            for cp in loads[3:]:
-                cp.wait()
-
-        @pl.when(t == 3)
-        def _():
-            mixer_finish()
-
-        @pl.when((t >= 2) & (t < nz + 2))
-        def _():
-            compute(t - 2)
-
-        @pl.when((t >= 3) & (t < nz + 3))
+        @pl.when((t >= 3) & (t < units + 3))
         def _():
             k = t - 3
-            zs = zpeer(k)
+            zs = unit(k)
             arrived(rd.at[zs], r_o.at[zs])
             sx[zs] = (po[zs, c].astype(f32) + rd[zs].astype(f32)).astype(bf16)
             for j in range(1, nx):
                 sum_x(k, j).start()
 
+            @pl.when(k == units - 2)
+            def _():
+                for j in range(1, nx):
+                    mix_out(j, 0).start()
+
+            @pl.when(k == units - 1)
+            def _():
+                for j in range(1, nx):
+                    mix_out(j, 1).start()
+
         @pl.when(t >= 4)
         def _():
             k = t - 4
-            zs = zpeer(k)
+            zs = unit(k)
             total = sx[zs, x].astype(f32)
             for j in range(1, nx):
                 arrived(rx.at[zs, xpeer(j)], r_p.at[zs, xpeer(j)])
                 total = total + rx[zs, xpeer(j)].astype(f32)
 
-            @pl.when(k == 0)
+            @pl.when(k < parts)
             def _():
-                ret[z] = total.astype(bf16)
-
-            @pl.when(k > 0)
+                ret[zs] = total.astype(bf16)
+
+            @pl.when(k >= parts)
             def _():
                 sz[zs] = total.astype(bf16)
                 back(k).start()
 
+        @pl.when(t == units // 2)
+        def _():
+            mixer_project()
+
+        @pl.when(t == units // 2 + 1)
+        def _():
+            mixer_finish()
+
+        @pl.when(t == 2)
+        def _():
+            for cp in loads[3:]:
+                cp.wait()
+
+        @pl.when((t >= 2) & (t < units + 2))
+        def _():
+            compute(t - 2)
+
         return 0
 
-    lax.fori_loop(0, nz + 4, step, 0)
+    lax.fori_loop(0, units + 4, step, 0)
 
     total = mo[x].astype(f32)
     for j in range(1, nx):
-        arrived(mr.at[xpeer(j)], r_q.at[xpeer(j)])
+        for h in range(2):
+            half = pl.ds(h * (own // 2), own // 2)
+            arrived(mr.at[xpeer(j), half], r_q.at[xpeer(j), h])
         total = total + mr[xpeer(j)].astype(f32)
     mixed[...] = total.astype(bf16)
 
-    for k in range(1, nz):
-        arrived(ret.at[zpeer(k)], r_b.at[zpeer(k)])
-    moe[...] = jnp.dot(mark[...], ret[...].reshape(nz * slots, d), preferred_element_type=f32).astype(bf16)
+    for k in range(parts, units):
+        arrived(ret.at[unit(k)], r_b.at[unit(k)])
+    moe[...] = jnp.dot(mark[...], ret[...].reshape(units * slots, d), preferred_element_type=f32).astype(bf16)
 
     rim().wait_send()
     for j in range(1, nx):
         mix_x(j).wait_send()
-        mix_out(j).wait_send()
-    for k in range(nz):
-        if k:
+        mix_out(j, 0).wait_send()
+        mix_out(j, 1).wait_send()
+    for k in range(units):
+        if k >= parts:
             send_z(k).wait_send()
             back(k).wait_send()
         pair(k).wait_send()
@@ -313,7 +338,9 @@
     nz = lax.axis_size("ep") // duo
     experts = held * lax.axis_size("ep")
     slots = (own * GROUP_SIZE // experts) * GROUP_SIZE // 2
-    dims = (nz, duo, nx, slots, own, d)
+    parts = PARTS if slots % (PARTS * 16) == 0 else 1
+    units, slots = nz * parts, slots // parts
+    dims = (nz, parts, duo, nx, slots, own, d)
     vmem, anyspace = pl.BlockSpec(memory_space=pltpu.VMEM), pl.BlockSpec(memory_space=pl.ANY)
     dma = pltpu.SemaphoreType.DMA
     down = expert_down.reshape(held * width, d)
@@ -322,17 +349,17 @@
     scratch = [
         V(proj_in.shape, bf16), V(pool_weight.shape, bf16), V(proj_out.shape, bf16),
         V(expert_gate.shape, bf16), V(expert_up.shape, bf16), V(down.shape, bf16),
-        V((own, d + MARK), bf16), V((own, nz * slots), bf16), V((nz, slots, d + MARK), bf16),
-        V((nz, duo, nx, slots, d + MARK), bf16), V((duo * nx * slots, held * width), bf16),
-        V((nz, duo, nx, slots, d), bf16), V((nz, nx, slots, d), bf16),
-        V((nz, nx, slots, d), bf16), V((nz, nx, slots, d), bf16),
-        V((nz, slots, d), bf16), V((nz, slots, d), bf16),
+        V((own, own), f32), V((own, d + MARK), bf16), V((own, units * slots), bf16), V((units, slots, d + MARK), bf16),
+        V((units, duo, nx, slots, d + MARK), bf16), V((duo * nx * slots, held * width), bf16),
+        V((units, duo, nx, slots, d), bf16), V((units, nx, slots, d), bf16),
+        V((units, nx, slots, d), bf16), V((units, nx, slots, d), bf16),
+        V((units, slots, d), bf16), V((units, slots, d), bf16),
         V((nx, own, d), bf16), V((HALO + nx * own, local), bf16),
         V((nx, own, d), bf16), V((nx, own, d), bf16),
-        dma((6,)), dma((nz,)), dma((nz,)),
-        dma((nz, nx)), dma((nz, nx)), dma((nz, nx)), dma((nz, nx)),
-        dma((nz,)), dma((nz,)), dma((nz, nx)), dma((nz, nx)), dma((nz,)), dma((nz,)),
-        dma((nx,)), dma((nx,)), dma, dma, dma((nx,)), dma((nx,)),
+        dma((6,)), dma((units,)), dma((units,)),
+        dma((units, nx)), dma((units, nx)), dma((units, nx)), dma((units, nx)),
+        dma((units,)), dma((units,)), dma((units, nx)), dma((units, nx)), dma((units,)), dma((units,)),
+        dma((nx,)), dma((nx,)), dma, dma, dma((nx, 2)), dma((nx, 2)),
     ]
     return pl.pallas_call(
         functools.partial(kernel, dims),
@@ -351,7 +378,7 @@
         ),
     )(
         mixer_tokens, mixer_gain.reshape(1, d), proj_in, pool_weight, pool_scale.reshape(1, local), proj_out,
-        expert_tokens, expert_gain.reshape(1, d), expert_route, route_gate, expert_gate, expert_up, down,
+        expert_tokens, expert_gain.reshape(1, d), expert_route.T, route_gate.T, expert_gate, expert_up, down,
     )
 
 

time: 100 us -> 87.6 us (0.88)
  Pallas kernels: 91.8 us -> 83 us
  local copies, waits for them, and re-layouts: 6.71 us -> 3.76 us
    pallas_call x1, Pallas kernels: 91.8 us -> 83 us  [shards(): pl.pallas_call(functools.partial(kernel, dims), out_shape=(jax.ShapeDtype...]
    unnamed x4 -> x2, local copies, waits for them, and re-layouts: 6.71 us -> 3.76 us
where the time goes in v2:
time: 87.6 us; the launch traced here: 87.4 us
  Pallas kernels  83 us (95%)
  local copies, waits for them, and re-layouts  3.76 us (4%)
    pallas_call x1, Pallas kernels, shards(): pl.pallas_call(functools.partial(kernel, dims), out_shape=(jax.ShapeDtype...  83 us
    unnamed x2, local copies, waits for them, and re-layouts  3.76 us

profile of v2, /device:TPU:0, one launch (start us, length us, event | category | flops | bytes accessed | tf_op | source)
XLA Modules:
  0.0 87.4 jit_solution(3700824431327690860)
XLA Ops:
  0.6 83.0 %shard_map.140 = (bf16[128,2048]{1,0:T(8,128)(2,1)}, bf16[128,2048]{1,0:T(8,128)(2,1)}) custom-call(bf16[128,2048]{1,0:T(8,128)(2,1)} %mixer.1, f32[1,2048]{1,0:T(1,128)} %bitcast.7, bf16[2048,512]{1,0:T(8,128)(2,1)} %proj_in.1, bf16[2,256,256]{2,1,0:T(8,128)(2,1)} %pool_w.1, f32[1,512]{1,0:T(1,128)} %bitcast.9, bf16[512,2048]{1,0:T(8,128)(2,1)} %proj_out.1, ...), custom_call_target="tpu_custom_call" | custom-call | tf_op jit(solution)/shard_map/pallas_call | solution.py:364
  83.6 1.9 %copy.17 = bf16[128,2048]{1,0:T(8,128)(2,1)} copy(bf16[128,2048]{1,0:T(8,128)(2,1)} %get-tuple-element.4) | data formatting | bytes 1048576
  85.5 1.9 %copy.18 = bf16[128,2048]{1,0:T(8,128)(2,1)} copy(bf16[128,2048]{1,0:T(8,128)(2,1)} %get-tuple-element.5) | data formatting | bytes 1048576
